TPU v7x, 128 devices: a whole 4x4x4 slice. The times are simulated.
128 devices in a mesh: dp: 4 (over x), kv: 16 (over z, y), tp: 2 (over core).
Axes of the slice: x: 4, y: 4, z: 4, core: 2. Of those that a mesh axis runs over, the one named last changes fastest.
Arguments:
- tokens: bfloat16 [512, 2048], P('dp', ('kv', 'tp')), may hold values from -100 to 100
- delta_state: float32 [512, 8, 128, 128], P(('dp', 'kv'), 'tp'), may hold values from -0.6 to 0.6
- gain_in: bfloat16 [2048], P('kv'), may hold values from 0.099609375 to 1.8984375
- w_query: bfloat16 [2048, 1024], P('kv', 'tp'), may hold values from -0.125 to 0.125
- w_key: bfloat16 [2048, 1024], P('kv', 'tp'), may hold values from -0.125 to 0.125
- w_value: bfloat16 [2048, 1024], P('kv', 'tp'), may hold values from -0.125 to 0.125
- w_out_gate: bfloat16 [2048, 1024], P('kv', 'tp'), may hold values from -0.125 to 0.125
- w_beta: bfloat16 [2048, 8], P('kv'), may hold values from -0.125 to 0.125
- w_decay: bfloat16 [2048, 8], P('kv'), may hold values from -0.125 to 0.125
- decay_rate: float32 [8], P('tp'), may hold values from 0.05 to 3
- head_gain: float32 [128], replicated, may hold values from 0.1 to 1.9
- w_mix: bfloat16 [1024, 2048], P('tp', 'kv'), may hold values from -0.1875 to 0.1875
- gain_mid: bfloat16 [2048], P('kv'), may hold values from 0.099609375 to 1.8984375
- w_gate: bfloat16 [2048, 5632], P('tp', 'kv'), may hold values from -0.125 to 0.125
- w_up: bfloat16 [2048, 5632], P('tp', 'kv'), may hold values from -0.125 to 0.125
- w_down: bfloat16 [5632, 2048], P('kv', 'tp'), may hold values from -0.078125 to 0.078125
Outputs:
- layer_out: bfloat16 [512, 2048], P('dp', ('kv', 'tp'))
- next_state: float32 [512, 8, 128, 128], P(('dp', 'kv'), 'tp')
All inputs are finite; a program needn't handle non-finite values.
Results may differ from a plain program's by a relative error of at most 0.0095.
Values may be sent and summed in bfloat16 or wider, within the bound.
No kernel may reach another device: no remote copies, remote signals or barrier semaphores. Data moves between devices by JAX's collectives and lax.ppermute only.
A program may use at most 64 MiB of HBM per device.

v0:
```python
import jax
import jax.numpy as jnp
from jax import lax
from jax.experimental import pallas as pl
from jax.experimental.pallas import tpu as pltpu
from jax.sharding import Mesh
from jax.sharding import PartitionSpec as P


D = 2048
HEAD_DIM = 128
KV = ("kv_0", "kv_1")
KV_TP = ("kv_0", "kv_1", "tp")
DP_KV = ("dp", "kv_0", "kv_1")

norm_epsilon = 1e-06
bf16 = jnp.bfloat16
f32 = jnp.float32

GROUP = 16
ROWS = 128
OWN = ROWS // GROUP
FEAT = 64
HEADS_DEV = 4
WIDTH_DEV = HEADS_DEV * HEAD_DIM
SMALL_AT = 4 * WIDTH_DEV
PIECE = SMALL_AT + 128
RING = 4
FEAT_RING = RING * FEAT
SEQ_RING = RING * OWN
PACKED = WIDTH_DEV + SEQ_RING
JOINED = 2 * WIDTH_DEV + SEQ_RING
HIDDEN = 352
BOTH = 2 * HIDDEN

TN = (((0,), (0,)), ((), ()))
NT = (((1,), (1,)), ((), ()))


def in_vmem():
    return pl.BlockSpec(memory_space=pltpu.VMEM)


def anywhere():
    return pl.BlockSpec(memory_space=pl.ANY)


def shape(lengths, dtype):
    return jax.ShapeDtypeStruct(lengths, dtype)


def kernel(body, outs, in_specs, limit=12):
    single = not isinstance(outs, (list, tuple))
    return pl.pallas_call(
        body,
        out_shape=outs,
        in_specs=in_specs,
        out_specs=in_vmem() if single else [in_vmem() for _ in outs],
        compiler_params=pltpu.CompilerParams(vmem_limit_bytes=limit * 1024 * 1024),
    )


def silu(value):
    return value / (1.0 + jnp.exp(-value))


def high_low(value):
    high = value.astype(bf16).astype(f32)
    return high, value - high


def dot(left, right, dims=(((1,), (0,)), ((), ()))):
    return lax.dot_general(left, right, dims, preferred_element_type=f32)


def half_turn(value):
    return pltpu.roll(value, 64, 1)


def project(
    own_ref, gain_ref, gain_mid_ref, wq_ref, wk_ref, wv_ref, wg_ref, wb_ref, wd_ref, other_ref, out_ref, rows_ref
):
    on_first = lax.axis_index("tp") == 0
    own = own_ref[...].astype(f32)
    other = other_ref[...].astype(f32)
    rows = jnp.concatenate(
        [jnp.where(on_first, own, other), jnp.where(on_first, other, own)], axis=0
    ).T
    rows_ref[...] = rows.astype(bf16)
    high, low = high_low(jnp.sum(rows * rows, axis=1, keepdims=True))
    normed = (rows * gain_ref[...].astype(f32)).astype(bf16)
    for at, ref in enumerate((wq_ref, wk_ref, wv_ref, wg_ref)):
        out_ref[:, at * WIDTH_DEV : (at + 1) * WIDTH_DEV] = dot(normed, ref[...]).astype(bf16)
    beta = wb_ref[...].astype(f32)
    decay = wd_ref[...].astype(f32)
    small = jnp.concatenate(
        [
            jnp.where(on_first, beta[:HEADS_DEV], beta[HEADS_DEV:]),
            jnp.where(on_first, decay[:HEADS_DEV], decay[HEADS_DEV:]),
            jnp.zeros((128 - 2 * HEADS_DEV, 128), f32),
        ],
        axis=0,
    ).astype(bf16)
    extra = dot(normed, small, NT)
    lane = lax.broadcasted_iota(jnp.int32, extra.shape, 1)
    gain_mid = jnp.broadcast_to(gain_mid_ref[...].astype(f32), extra.shape)
    gain_mid = jnp.where(on_first, half_turn(gain_mid), gain_mid)
    extra = jnp.where(lane == 2 * HEADS_DEV, high, extra)
    extra = jnp.where(lane == 2 * HEADS_DEV + 1, low, extra)
    out_ref[:, SMALL_AT:] = jnp.where(lane >= 64, gain_mid, extra).astype(bf16)


def low_lanes(value):
    return lax.broadcasted_iota(jnp.int32, value.shape, 1) < 64


def ring_tokens(rows_ref, place, on_first, low):
    parts = [
        rows_ref[pl.ds(pl.multiple_of(SEQ_RING * r + OWN * place, OWN), OWN)].astype(f32)
        for r in range(RING)
    ]
    value = jnp.concatenate(parts, axis=0)
    turned = half_turn(value)
    return jnp.where(on_first, value, turned) if low else jnp.where(on_first, turned, value)


def pack(own_ref, other_ref, rows_ref, out_ref):
    on_first = lax.axis_index("tp") == 0
    place = lax.axis_index("kv_1")
    own = own_ref[...].astype(f32)
    other = other_ref[...].astype(f32)
    top = jnp.where(on_first, own, half_turn(other))
    bottom = jnp.where(on_first, half_turn(other), own)
    out_ref[:WIDTH_DEV] = jnp.where(low_lanes(own), top, bottom).astype(bf16)
    first = ring_tokens(rows_ref, jnp.bitwise_xor(place, 3), on_first, True)
    second = ring_tokens(rows_ref, jnp.bitwise_xor(place, 2), on_first, False)
    out_ref[WIDTH_DEV:] = jnp.where(low_lanes(first), first, second).astype(bf16)


def mixer(
    pieces_ref,
    state_ref,
    rate_ref,
    head_gain_ref,
    mixed_ref,
    key_ref,
    correct_ref,
    keep_ref,
    gain_ref,
):
    def total(first, last):
        parts = [pieces_ref[OWN * s : OWN * (s + 1), first:last].astype(f32) for s in range(GROUP)]
        while len(parts) > 1:
            parts = [a + b for a, b in zip(parts[::2], parts[1::2])]
        return parts[0]

    def block(s, at):
        return pieces_ref[OWN * s : OWN * (s + 1), at : at + 128].astype(f32)

    small = total(SMALL_AT, PIECE)
    lane = lax.broadcasted_iota(jnp.int32, (OWN, HEAD_DIM), 1)
    squares = jnp.where((lane == 2 * HEADS_DEV) | (lane == 2 * HEADS_DEV + 1), small, 0.0)
    row_scale = lax.rsqrt(jnp.sum(squares, axis=1, keepdims=True) / D + norm_epsilon)
    small = small * row_scale
    own = jnp.bitwise_and(lax.broadcasted_iota(jnp.int32, (2 * OWN, HEAD_DIM), 0), OWN - 1)
    keeps = jnp.zeros((OWN, HEAD_DIM), f32)
    low = lane < 64
    for s in range(0, GROUP, 2):
        gain_ref[:, FEAT * s : FEAT * (s + 2)] = jnp.where(
            low, half_turn(block(s, SMALL_AT)), block(s + 1, SMALL_AT)
        )

    def unit(vector):
        return vector * lax.rsqrt(jnp.sum(vector * vector, axis=1, keepdims=True) + norm_epsilon)

    for h in range(HEADS_DEV):
        at = h * HEAD_DIM
        query_lin, key_lin, value_lin, gate_lin = (
            total(part * WIDTH_DEV + at, part * WIDTH_DEV + at + HEAD_DIM) * row_scale
            for part in range(4)
        )
        query = unit(silu(query_lin)) * HEAD_DIM ** (-0.5)
        key = unit(silu(key_lin))
        write_rate = 1.0 / (1.0 + jnp.exp(-small[:, h : h + 1]))
        decay = small[:, HEADS_DEV + h : HEADS_DEV + h + 1]
        softplus = jnp.maximum(decay, 0.0) + jnp.log1p(jnp.exp(-jnp.abs(decay)))
        keep = jnp.exp(-rate_ref[:, h : h + 1] * softplus)
        pair = jnp.concatenate([key, query], axis=0)
        spread = jnp.concatenate([jnp.where(own == b, pair, 0.0) for b in range(OWN)], axis=1)
        states = state_ref[:, h].reshape(OWN * HEAD_DIM, HEAD_DIM)
        both = dot(spread.astype(bf16), states.astype(bf16))
        recalled, asked = both[:OWN], both[OWN:]
        correction = write_rate * (silu(value_lin) - keep * recalled)
        readout = keep * asked + jnp.sum(key * query, axis=1, keepdims=True) * correction
        readout = readout * lax.rsqrt(
            jnp.mean(readout * readout, axis=1, keepdims=True) + norm_epsilon
        )
        mixed = (readout * head_gain_ref[...] * silu(gate_lin)).astype(bf16)
        for e in range(2 * RING):
            mixed_ref[OWN * e : OWN * (e + 1), at : at + HEAD_DIM] = mixed
        key_ref[:, at : at + HEAD_DIM] = key
        correct_ref[:, at : at + HEAD_DIM] = correction
        keeps = jnp.where(lane == h, keep, keeps)
    keep_ref[...] = keeps


def update(state_ref, key_ref, correct_ref, keep_ref, after_ref, next_ref, token_ref, made_ref, sems):
    del after_ref
    copies = []
    for b in range(OWN):
        for h in range(HEADS_DEV):
            at = h * HEAD_DIM
            key_column = jnp.broadcast_to(key_ref[b : b + 1, at : at + HEAD_DIM], (128, 128)).T
            made_ref[b, h] = (
                keep_ref[b : b + 1, h : h + 1] * state_ref[b, h]
                + key_column * correct_ref[b : b + 1, at : at + HEAD_DIM]
            )
        copies.append(pltpu.make_async_copy(made_ref.at[b], next_ref.at[b], sems.at[b]))
        copies[-1].start()
    token_ref[...] = jnp.zeros(token_ref.shape, f32)
    for copy in copies:
        copy.wait()


def updated(*operands):
    return pl.pallas_call(
        update,
        out_shape=[shape(operands[0].shape, f32), shape((8, 128), f32)],
        in_specs=[in_vmem()] * 4 + [anywhere()],
        out_specs=[pl.BlockSpec(memory_space=pltpu.HBM), in_vmem()],
        scratch_shapes=[
            pltpu.VMEM((OWN, HEADS_DEV, HEAD_DIM, HEAD_DIM), f32),
            pltpu.SemaphoreType.DMA((OWN,)),
        ],
        name="update",
        compiler_params=pltpu.CompilerParams(vmem_limit_bytes=12 * 1024 * 1024),
    )(*operands)


def preload(*refs):
    count = (len(refs) - 1) // 2
    sems = refs[-1]
    copies = [
        pltpu.make_async_copy(refs[i], refs[count + i], sems.at[i]) for i in range(count)
    ]
    for copy in copies:
        copy.start()
    for copy in copies:
        copy.wait()


def preloaded(*arrays):
    return pl.pallas_call(
        preload,
        out_shape=[shape(x.shape, x.dtype) for x in arrays],
        in_specs=[pl.BlockSpec(memory_space=pltpu.HBM)] * len(arrays),
        out_specs=[in_vmem() for _ in arrays],
        scratch_shapes=[pltpu.SemaphoreType.DMA((len(arrays),))],
        name="preload",
        compiler_params=pltpu.CompilerParams(vmem_limit_bytes=4 * 1024 * 1024),
    )(*(pltpu.with_memory_space_constraint(x, pltpu.HBM) for x in arrays))


def note(after_ref, out_ref):
    del after_ref
    out_ref[...] = jnp.zeros(out_ref.shape, f32)


def join(held_ref, near_ref, rows_ref, after_ref, out_ref):
    del after_ref
    on_first = lax.axis_index("tp") == 0
    place = lax.axis_index("kv_1")
    out_ref[:WIDTH_DEV] = held_ref[:WIDTH_DEV]
    out_ref[WIDTH_DEV : 2 * WIDTH_DEV] = near_ref[:WIDTH_DEV]
    first = ring_tokens(rows_ref, jnp.bitwise_xor(place, 1), on_first, True)
    second = near_ref[WIDTH_DEV:].astype(f32)
    out_ref[2 * WIDTH_DEV :] = jnp.where(low_lanes(first), first, second).astype(bf16)


def ring_parts(received_ref, joined_ref):
    mixed = jnp.concatenate(
        [
            received_ref[OWN * (2 * r + core) : OWN * (2 * r + core + 1)].astype(f32)
            for core in range(2)
            for r in range(RING)
        ],
        axis=0,
    ).astype(bf16)
    parts = []
    for at in (0, WIDTH_DEV):
        both = dot(mixed, joined_ref[at : at + WIDTH_DEV])
        parts.append(both[:SEQ_RING] + half_turn(both[SEQ_RING:]))
    return parts


def mix(received_ref, joined_ref, near_ref, far_ref, rows_ref, after_ref, sent_ref):
    del after_ref
    on_first = lax.axis_index("tp") == 0
    place = lax.axis_index("kv_1")
    held, third = ring_parts(received_ref, joined_ref)
    first, second = ring_parts(received_ref, far_ref)
    far_tokens = far_ref[2 * WIDTH_DEV :].astype(f32)
    parts = [
        held + ring_tokens(rows_ref, place, on_first, True),
        first + far_tokens,
        second + half_turn(far_tokens),
        third + near_ref[WIDTH_DEV:].astype(f32),
    ]

    def part(column):
        which = jnp.bitwise_xor(place, column)
        value = parts[0]
        for m in range(1, RING):
            value = jnp.where(which == m, parts[m], value)
        return value

    low = low_lanes(parts[0])
    middle = jnp.concatenate(
        [jnp.where(low, part(c), half_turn(part(c + 1))) for c in range(0, RING, 2)], axis=1
    ).astype(bf16)
    for s in range(GROUP):
        sent_ref[SEQ_RING * s : SEQ_RING * (s + 1)] = middle


def gate_up(received_ref, gain_ref, wg_ref, wu_ref, own_ref, sent_ref, middle_ref, rows_ref):
    for s in range(GROUP):
        ring, place = s // RING, s % RING
        for r in range(RING):
            rows_ref[
                SEQ_RING * r + OWN * place : SEQ_RING * r + OWN * (place + 1),
                FEAT_RING * ring : FEAT_RING * (ring + 1),
            ] = received_ref[SEQ_RING * s + OWN * r : SEQ_RING * s + OWN * (r + 1)]
    middle = rows_ref[...].astype(f32)
    normed = (middle * gain_ref[0:1]).astype(bf16)
    for at, ref in ((0, wg_ref), (HIDDEN, wu_ref)):
        value = dot(ref[...], normed, NT)
        own_ref[at : at + HIDDEN] = value
        sent_ref[at : at + HIDDEN] = value.astype(bf16)
    squares = jnp.sum(middle * middle, axis=1, keepdims=True)
    total = jnp.broadcast_to(squares, (ROWS, 128)).T[0:1]
    high, low = high_low(total)
    own_ref[BOTH:] = jnp.broadcast_to(total, (8, ROWS))
    sent_ref[BOTH:] = jnp.concatenate([high, low, jnp.zeros((6, ROWS), f32)], axis=0).astype(bf16)
    place = lax.axis_index("kv_1")
    pair = lax.axis_index("kv_0") * 2 + jnp.right_shift(place, 1)
    block = rows_ref[:, pl.ds(pl.multiple_of(pair * 128, 128), 128)].astype(f32).T
    even = jnp.bitwise_and(place, 1) == 0
    middle_ref[...] = jnp.where(even, block[:FEAT], block[FEAT:]).astype(bf16)


def down(own_ref, other_ref, w_ref, after_ref, out_ref):
    del after_ref
    squares = other_ref[BOTH:].astype(f32)
    total = own_ref[BOTH : BOTH + 1] + squares[0:1] + squares[1:2]
    scale = lax.rsqrt(total / D + norm_epsilon)
    gate = (own_ref[:HIDDEN] + other_ref[:HIDDEN].astype(f32)) * scale
    up = (own_ref[HIDDEN:BOTH] + other_ref[HIDDEN:BOTH].astype(f32)) * scale
    active = (silu(gate) * up).astype(bf16)
    out_ref[...] = dot(w_ref[...], active, TN).astype(bf16)


def finish(received_ref, middle_ref, out_ref):
    parts = [received_ref[FEAT * s : FEAT * (s + 1)].astype(f32) for s in range(GROUP)]
    while len(parts) > 1:
        parts = [a + b for a, b in zip(parts[::2], parts[1::2])]
    out_ref[...] = (middle_ref[...].astype(f32) + parts[0]).astype(bf16)


def from_other_core(array):
    return lax.ppermute(array, "tp", [(0, 1), (1, 0)])


def over(array, axes, members):
    tiles = array.reshape(members, array.shape[0] // members, array.shape[1])
    return lax.all_to_all(tiles, axes, 0, 0, tiled=True).reshape(array.shape)


def from_ring(array, flip):
    return lax.ppermute(array, "kv_1", [(i, i ^ flip) for i in range(RING)])


def layer(
    tokens,
    delta_state,
    gain_in,
    w_query,
    w_key,
    w_value,
    w_out_gate,
    w_beta,
    w_decay,
    decay_rate,
    head_gain,
    w_mix,
    gain_mid,
    w_gate,
    w_up,
    w_down,
):
    v, a = in_vmem(), anywhere()
    own_tokens = tokens.T
    other_tokens = from_other_core(own_tokens)
    other_mix = from_other_core(w_mix)
    *loaded, own_mix = preloaded(
        own_tokens,
        gain_in.reshape(1, 128),
        gain_mid.reshape(1, 128),
        w_query,
        w_key,
        w_value,
        w_out_gate,
        w_beta.T,
        w_decay.T,
        w_mix,
    )
    summand, rows = kernel(
        project, [shape((ROWS, PIECE), bf16), shape((ROWS, 128), bf16)], [v] * 10
    )(*loaded, other_tokens)
    held = kernel(pack, shape((PACKED, 128), bf16), [v] * 3)(own_mix, other_mix, rows)
    near = from_ring(held, 3)
    pieces = over(summand, KV, GROUP)
    mark = kernel(note, shape((8, 128), f32), [a])(pieces)
    joined = kernel(join, shape((JOINED, 128), bf16), [v] * 3 + [a])(
        held, near, rows, mark
    )
    far = from_ring(joined, 1)
    mixed, key, correction, keep, gains = kernel(
        mixer,
        [
            shape((2 * RING * OWN, WIDTH_DEV), bf16),
            shape((OWN, WIDTH_DEV), f32),
            shape((OWN, WIDTH_DEV), f32),
            shape((OWN, HEAD_DIM), f32),
            shape((OWN, GROUP * FEAT), f32),
        ],
        [v] * 4,
    )(pieces, delta_state, decay_rate.reshape(1, HEADS_DEV), head_gain.reshape(1, HEAD_DIM))
    mixed_rows = over(mixed, ("kv_0", "tp"), 2 * RING)
    arrived = kernel(note, shape((8, 128), f32), [a])(mixed_rows)
    sent = kernel(mix, shape((GROUP * SEQ_RING, FEAT_RING), bf16), [v] * 5 + [a])(
        mixed_rows, joined, near, far, rows, arrived
    )
    received = over(sent, KV, GROUP)
    own_sum, sent_sum, middle = pl.pallas_call(
        gate_up,
        out_shape=[
            shape((BOTH + 8, ROWS), f32),
            shape((BOTH + 8, ROWS), bf16),
            shape((FEAT, ROWS), bf16),
        ],
        in_specs=[v] * 4,
        out_specs=[v] * 3,
        scratch_shapes=[pltpu.VMEM((ROWS, GROUP * FEAT), bf16)],
        name="gate_up",
        compiler_params=pltpu.CompilerParams(vmem_limit_bytes=12 * 1024 * 1024),
    )(received, gains, w_gate.T, w_up.T)
    next_state, token = updated(delta_state, key, correction, keep, received)
    down_local = kernel(down, shape((GROUP * FEAT, ROWS), bf16), [v, v, v, a])(
        own_sum, from_other_core(sent_sum), w_down, token
    )
    layer_out = kernel(finish, shape((FEAT, ROWS), bf16), [v] * 2)(
        over(down_local, KV, GROUP), middle
    )
    return (layer_out.T, next_state)


def solution(mesh):
    split = Mesh(
        mesh.devices.reshape(mesh.shape["dp"], 4, 4, mesh.shape["tp"]), ("dp", "kv_0", "kv_1", "tp")
    )
    in_specs = (
        P("dp", KV_TP),
        P(DP_KV, "tp", None, None),
        P(KV),
        P(KV, "tp"),
        P(KV, "tp"),
        P(KV, "tp"),
        P(KV, "tp"),
        P(KV, None),
        P(KV, None),
        P("tp"),
        P(),
        P("tp", KV),
        P(KV),
        P("tp", KV),
        P("tp", KV),
        P(KV, "tp"),
    )
    out_specs = (P("dp", KV_TP), P(DP_KV, "tp", None, None))
    return jax.shard_map(layer, mesh=split, in_specs=in_specs, out_specs=out_specs, check_vma=False)
```

profile of v0, /device:TPU:1, one launch (start us, length us, event | category | flops | bytes accessed | tf_op | source)
XLA Modules:
  0.0 63.6 jit_solution(10544231218129492202)
XLA Ops:
  0.7 1.5 %collective-permute-start = (bf16[64,128]{1,0:T(8,128)(2,1)}, bf16[64,128]{1,0:T(8,128)(2,1)S(1)}, u32[]{:S(2)}, u32[]{:S(2)}) collective-permute-start(bf16[64,128]{1,0:T(8,128)(2,1)} %bitcast.33), channel_id=1, source_target_pairs={{0,1},{1,0},{2,3},{3,2},{4,5},{5,4},{6,7},{7,6},{8,9},{9,8},{10,11... | collective-permute-start | bytes 49160 | tf_op jit(solution)/shard_map/ppermute | solution.py:370
  2.1 1.3 %preload.1 = (bf16[64,128]{1,0:T(8,128)(2,1)S(1)}, bf16[1,128]{1,0:T(2,128)(2,1)S(1)}, bf16[1,128]{1,0:T(2,128)(2,1)S(1)}, bf16[128,512]{1,0:T(8,128)(2,1)S(1)},...) custom-call(bf16[64,128]{1,0:T(8,128)(2,1)} %bitcast.34, ...), custom_call_target="tpu_custom_call" | custom-call | tf_op jit(solution)/shard_map/preload/pallas_call | solution.py:253
  3.5 1.2 %shard_map.167 = (bf16[128,2176]{1,0:T(8,128)(2,1)}, bf16[128,128]{1,0:T(8,128)(2,1)S(1)}) custom-call(bf16[64,128]{1,0:T(8,128)(2,1)S(1)} %get-tuple-element.24.own_ref, bf16[1,128]{1,0:T(2,128)(2,1)S(1)} %get-tuple-element.25.gain_ref, bf16[1,128]{1,0:T(2,128)(2,1)S(1)} %get-tuple-element.26.gain_mid_ref, bf16[128,512]{1,0:T(8,128)(2,1)S(1)} %get-tuple-element.27.wq_ref, ...), custom_call_target="tpu_custom_call" | custom-call | tf_op jit(solution)/shard_map/pallas_call | solution.py:416
  4.6 7.9 %all-to-all-start = ((bf16[16,8,2176]{2,1,0:T(8,128)(2,1)}), bf16[16,8,2176]{2,1,0:T(8,128)(2,1)S(1)}, u32[]{:S(2)}, u32[]{:S(2)}) async-start(bf16[16,8,2176]{2,1,0:T(8,128)(2,1)} %bitcast.5), calls=%async_computation | async-start | bytes 1114112 | tf_op jit(solution)/shard_map/all_to_all | solution.py:375
  12.5 0.5 collective-permute-start.1
  13.1 1.0 %collective-permute-done.1.other_ref = bf16[512,128]{1,0:T(8,128)(2,1)S(1)} collective-permute-done((bf16[512,128]{1,0:T(8,128)(2,1)S(1)}, bf16[512,128]{1,0:T(8,128)(2,1)S(1)}, u32[]{:S(2)}, u32[]{:S(2)}) %collective-permute-start.1) | collective-permute-done | bytes 131104 | tf_op jit(solution)/shard_map/ppermute | solution.py:370
  14.0 0.1 shard_map.169.held_ref
  14.2 2.9 %collective-permute-start.2 = (bf16[544,128]{1,0:T(8,128)(2,1)S(1)}, bf16[544,128]{1,0:T(8,128)(2,1)S(1)}, u32[]{:S(2)}, u32[]{:S(2)}) collective-permute-start(bf16[544,128]{1,0:T(8,128)(2,1)S(1)} %shard_map.169.held_ref), channel_id=1, source_target_pairs={{0,6},{2,4},{4,2},{6,0},{1,7},{3,5},{5,3},{7,1},{8,14},{10,12},{12... | collective-permute-start | bytes 417800 | tf_op jit(solution)/shard_map/ppermute | solution.py:379
  17.1 6.7 %all-to-all-done = bf16[16,8,2176]{2,1,0:T(8,128)(2,1)S(1)} async-done(((bf16[16,8,2176]{2,1,0:T(8,128)(2,1)}), bf16[16,8,2176]{2,1,0:T(8,128)(2,1)S(1)}, u32[]{:S(2)}, u32[]{:S(2)}) %all-to-all-start) | async-done | bytes 557088 | tf_op jit(solution)/shard_map/all_to_all | solution.py:375
  23.8 1.3 %collective-permute-done.2.near_ref = bf16[544,128]{1,0:T(8,128)(2,1)S(1)} collective-permute-done((bf16[544,128]{1,0:T(8,128)(2,1)S(1)}, bf16[544,128]{1,0:T(8,128)(2,1)S(1)}, u32[]{:S(2)}, u32[]{:S(2)}) %collective-permute-start.2) | collective-permute-done | bytes 139296 | tf_op jit(solution)/shard_map/ppermute | solution.py:379
  25.1 0.1 shard_map.171.joined_ref
  25.2 0.0 collective-permute-start.3
  25.3 0.0 copy-start.1
  25.3 0.0 copy-start.2
  25.3 0.5 shard_map.168
  25.8 9.9 %all_to_all.20 = bf16[8,8,512]{2,1,0:T(8,128)(2,1)S(1)} all-to-all(bf16[8,8,512]{2,1,0:T(8,128)(2,1)S(1)} %bitcast.29), channel_id=1, replica_groups=mesh['dp'=4,'kv_0'=4,'kv_1'=4,'tp'=2] {'kv_0','tp'}, dimensions={0} | all-to-all | bytes 131072 | tf_op jit(solution)/shard_map/all_to_all | solution.py:375
  35.7 0.4 shard_map.173
  36.1 10.8 %all_to_all.21 = bf16[16,32,256]{2,1,0:T(8,128)(2,1)S(1)} all-to-all(bf16[16,32,256]{2,1,0:T(8,128)(2,1)S(1)} %bitcast.23), channel_id=1, replica_groups=mesh['dp'=4,'kv_0'=4,'kv_1'=4,'tp'=2] {'kv_0','kv_1'}, dimensions={0} | all-to-all | bytes 524288 | tf_op jit(solution)/shard_map/all_to_all | solution.py:375
  46.9 0.6 gate_up.1
  47.5 2.3 %collective-permute-start.4 = (bf16[712,128]{1,0:T(8,128)(2,1)S(1)}, bf16[712,128]{1,0:T(8,128)(2,1)S(1)}, u32[]{:S(2)}, u32[]{:S(2)}) collective-permute-start(bf16[712,128]{1,0:T(8,128)(2,1)S(1)} %get-tuple-element.39), channel_id=1, source_target_pairs={{0,1},{1,0},{2,3},{3,2},{4,5},{5,4},{6,7},{7,6},{8,9},{9,8},{10,11... | collective-permute-start | bytes 546824 | tf_op jit(solution)/shard_map/ppermute | solution.py:370
  49.8 1.6 %update.1 = (f32[8,4,128,128]{3,2,1,0:T(8,128)}, f32[8,128]{1,0:T(8,128)S(1)}) custom-call(f32[8,4,128,128]{3,2,1,0:T(8,128)S(1)} %copy-done, f32[8,512]{1,0:T(8,128)S(1)} %get-tuple-element.40.key_ref, f32[8,512]{1,0:T(8,128)S(1)} %get-tuple-element.41.correct_ref, f32[8,128]{1,0:T(8,128)S(1)} %get-tuple-element.42.keep_ref, bf16[512,256]{1,0:T(8,128)(2,1)S(1)} %bitcast.21), custom_call_target="tpu_custom_call" | custom-call | tf_op jit(solution)/shard_map/update/pallas_call | solution.py:226
  51.3 0.4 shard_map.174
  51.8 11.1 %all_to_all.22 = bf16[16,64,128]{2,1,0:T(8,128)(2,1)S(1)} all-to-all(bf16[16,64,128]{2,1,0:T(8,128)(2,1)S(1)} %bitcast.24), channel_id=1, replica_groups=mesh['dp'=4,'kv_0'=4,'kv_1'=4,'tp'=2] {'kv_0','kv_1'}, dimensions={0} | all-to-all | bytes 524288 | tf_op jit(solution)/shard_map/all_to_all | solution.py:375
  62.9 0.6 %shard_map.175 = bf16[64,128]{1,0:T(8,128)(2,1)} custom-call(bf16[1024,128]{1,0:T(8,128)(2,1)S(1)} %bitcast.22, bf16[64,128]{1,0:T(8,128)(2,1)S(1)} %get-tuple-element.44.middle_ref), custom_call_target="tpu_custom_call" | custom-call | tf_op jit(solution)/shard_map/pallas_call | solution.py:461
  (17 shorter events, 0.0 us)
Async XLA Ops:
  0.6 11.9 %copy-start.6 = (bf16[512,128]{1,0:T(8,128)(2,1)S(1)}, bf16[512,128]{1,0:T(8,128)(2,1)}, u32[]{:S(2)}) copy-start(bf16[512,128]{1,0:T(8,128)(2,1)} %refs_9_.1) | copy-start | bytes 393220
  0.6 24.6 %copy-start.4 = (f32[4]{0:T(128)S(1)}, f32[4]{0:T(128)}, u32[]{:S(2)}) copy-start(f32[4]{0:T(128)} %param.25) | copy-start | bytes 52
  0.7 24.6 %copy-start.5 = (f32[128]{0:T(128)S(1)}, f32[128]{0:T(128)}, u32[]{:S(2)}) copy-start(f32[128]{0:T(128)} %param.26) | copy-start | bytes 1540
  0.7 24.6 %copy-start = (f32[8,4,128,128]{3,2,1,0:T(8,128)S(1)}, f32[8,4,128,128]{3,2,1,0:T(8,128)}, u32[]{:S(2)}) copy-start(f32[8,4,128,128]{3,2,1,0:T(8,128)} %state_ref.3) | copy-start | bytes 6291460
  0.7 2.8 %collective-permute-start = (bf16[64,128]{1,0:T(8,128)(2,1)}, bf16[64,128]{1,0:T(8,128)(2,1)S(1)}, u32[]{:S(2)}, u32[]{:S(2)}) collective-permute-start(bf16[64,128]{1,0:T(8,128)(2,1)} %bitcast.33), channel_id=1, source_target_pairs={{0,1},{1,0},{2,3},{3,2},{4,5},{5,4},{6,7},{7,6},{8,9},{9,8},{10,11... | collective-permute-start | bytes 49160 | tf_op jit(solution)/shard_map/ppermute | solution.py:370
  4.6 19.1 %all-to-all-start = ((bf16[16,8,2176]{2,1,0:T(8,128)(2,1)}), bf16[16,8,2176]{2,1,0:T(8,128)(2,1)S(1)}, u32[]{:S(2)}, u32[]{:S(2)}) async-start(bf16[16,8,2176]{2,1,0:T(8,128)(2,1)} %bitcast.5), calls=%async_computation | async-start | bytes 1114112 | tf_op jit(solution)/shard_map/all_to_all | solution.py:375
  12.5 1.5 %collective-permute-start.1 = (bf16[512,128]{1,0:T(8,128)(2,1)S(1)}, bf16[512,128]{1,0:T(8,128)(2,1)S(1)}, u32[]{:S(2)}, u32[]{:S(2)}) collective-permute-start(bf16[512,128]{1,0:T(8,128)(2,1)S(1)} %copy-done.6), channel_id=1, source_target_pairs={{0,1},{1,0},{2,3},{3,2},{4,5},{5,4},{6,7},{7,6},{8,9},{9,8},{10,11... | collective-permute-start | bytes 393224 | tf_op jit(solution)/shard_map/ppermute | solution.py:370
  14.2 10.9 %collective-permute-start.2 = (bf16[544,128]{1,0:T(8,128)(2,1)S(1)}, bf16[544,128]{1,0:T(8,128)(2,1)S(1)}, u32[]{:S(2)}, u32[]{:S(2)}) collective-permute-start(bf16[544,128]{1,0:T(8,128)(2,1)S(1)} %shard_map.169.held_ref), channel_id=1, source_target_pairs={{0,6},{2,4},{4,2},{6,0},{1,7},{3,5},{5,3},{7,1},{8,14},{10,12},{12... | collective-permute-start | bytes 417800 | tf_op jit(solution)/shard_map/ppermute | solution.py:379
  25.2 10.5 %collective-permute-start.3 = (bf16[1056,128]{1,0:T(8,128)(2,1)S(1)}, bf16[1056,128]{1,0:T(8,128)(2,1)S(1)}, u32[]{:S(2)}, u32[]{:S(2)}) collective-permute-start(bf16[1056,128]{1,0:T(8,128)(2,1)S(1)} %shard_map.171.joined_ref), channel_id=1, source_target_pairs={{0,2},{2,0},{4,6},{6,4},{1,3},{3,1},{5,7},{7,5},{8,10},{10,8},{12,... | collective-permute-start | bytes 811016 | tf_op jit(solution)/shard_map/ppermute | solution.py:379
  25.3 21.7 %copy-start.1 = (bf16[1024,352]{0,1:T(8,128)(2,1)S(1)}, bf16[1024,352]{0,1:T(8,128)(2,1)}, u32[]{:S(2)}) copy-start(bf16[1024,352]{0,1:T(8,128)(2,1)} %param.29) | copy-start | bytes 2162692
  25.3 21.7 %copy-start.2 = (bf16[1024,352]{0,1:T(8,128)(2,1)S(1)}, bf16[1024,352]{0,1:T(8,128)(2,1)}, u32[]{:S(2)}) copy-start(bf16[1024,352]{0,1:T(8,128)(2,1)} %param.30) | copy-start | bytes 2162692
  46.9 4.4 %copy-start.3 = (bf16[352,1024]{1,0:T(8,128)(2,1)S(1)}, bf16[352,1024]{1,0:T(8,128)(2,1)}, u32[]{:S(2)}) copy-start(bf16[352,1024]{1,0:T(8,128)(2,1)} %w_ref.1) | copy-start | bytes 2162692
  47.5 3.8 %collective-permute-start.4 = (bf16[712,128]{1,0:T(8,128)(2,1)S(1)}, bf16[712,128]{1,0:T(8,128)(2,1)S(1)}, u32[]{:S(2)}, u32[]{:S(2)}) collective-permute-start(bf16[712,128]{1,0:T(8,128)(2,1)S(1)} %get-tuple-element.39), channel_id=1, source_target_pairs={{0,1},{1,0},{2,3},{3,2},{4,5},{5,4},{6,7},{7,6},{8,9},{9,8},{10,11... | collective-permute-start | bytes 546824 | tf_op jit(solution)/shard_map/ppermute | solution.py:370
where the time goes:
time: 63.9 us; the launch traced here: 63.6 us
  blocking collectives  31.9 us (50%)
  starting transfers between devices  15.1 us (24%)
  waiting for transfers between devices  9 us (14%)
  Pallas kernels  6.8 us (11%)
  between operations  0.81 us (1%)
    all_to_all x3, blocking collectives, over(): return lax.all_to_all(tiles, axes, 0, 0, tiled=True).reshape(array.shape)  31.9 us
    all_to_all x1, starting transfers between devices, over(): return lax.all_to_all(tiles, axes, 0, 0, tiled=True).reshape(array.shape)  7.88 us
    all_to_all x1, waiting for transfers between devices, over(): return lax.all_to_all(tiles, axes, 0, 0, tiled=True).reshape(array.shape)  6.66 us
    ppermute x3, starting transfers between devices, from_other_core(): return lax.ppermute(array, 'tp', [(0, 1), (1, 0)])  4.26 us
    ppermute x2, starting transfers between devices, from_ring(): return lax.ppermute(array, 'kv_1', [(i, i ^ flip) for i in range(RING)])  2.96 us
    pallas_call x1, Pallas kernels, updated(): pl.pallas_call(update, out_shape=[shape(operands[0].shape, f32), shape((8...  1.56 us
    ppermute x2, waiting for transfers between devices, from_ring(): return lax.ppermute(array, 'kv_1', [(i, i ^ flip) for i in range(RING)])  1.34 us
    pallas_call x1, Pallas kernels, preloaded(): pl.pallas_call(preload, out_shape=[shape(x.shape, x.dtype) for x in array...  1.31 us
  transfers between devices with their start and end apart: 6, of which 3 were waited for; matrix products, arithmetic and copies ran while one was open for 0% of the time, Pallas kernels for 6%

commit v1 on v0

--- a/solution.py
+++ b/solution.py
@@ -78,7 +78,7 @@
 
 
 def project(
-    own_ref, gain_ref, gain_mid_ref, wq_ref, wk_ref, wv_ref, wg_ref, wb_ref, wd_ref, other_ref, out_ref, rows_ref
+    own_ref, gain_ref, gain_mid_ref, wq_ref, wk_ref, wv_ref, wg_ref, wb_ref, wd_ref, own_mix_ref, other_ref, other_mix_ref, out_ref, rows_ref, held_ref
 ):
     on_first = lax.axis_index("tp") == 0
     own = own_ref[...].astype(f32)
@@ -108,6 +108,7 @@
     extra = jnp.where(lane == 2 * HEADS_DEV, high, extra)
     extra = jnp.where(lane == 2 * HEADS_DEV + 1, low, extra)
     out_ref[:, SMALL_AT:] = jnp.where(lane >= 64, gain_mid, extra).astype(bf16)
+    pack(own_mix_ref, other_mix_ref, rows_ref, held_ref)
 
 
 def low_lanes(value):
@@ -401,7 +402,7 @@
     own_tokens = tokens.T
     other_tokens = from_other_core(own_tokens)
     other_mix = from_other_core(w_mix)
-    *loaded, own_mix = preloaded(
+    loaded = preloaded(
         own_tokens,
         gain_in.reshape(1, 128),
         gain_mid.reshape(1, 128),
@@ -413,10 +414,11 @@
         w_decay.T,
         w_mix,
     )
-    summand, rows = kernel(
-        project, [shape((ROWS, PIECE), bf16), shape((ROWS, 128), bf16)], [v] * 10
-    )(*loaded, other_tokens)
-    held = kernel(pack, shape((PACKED, 128), bf16), [v] * 3)(own_mix, other_mix, rows)
+    summand, rows, held = kernel(
+        project,
+        [shape((ROWS, PIECE), bf16), shape((ROWS, 128), bf16), shape((PACKED, 128), bf16)],
+        [v] * 12,
+    )(*loaded, other_tokens, other_mix)
     near = from_ring(held, 3)
     pieces = over(summand, KV, GROUP)
     mark = kernel(note, shape((8, 128), f32), [a])(pieces)

time: 63.9 us -> 64 us (level)
  waiting for transfers between devices: 9 us -> 10 us
  starting transfers between devices: 15.1 us -> 14.3 us
    all_to_all x1, waiting for transfers between devices: 6.66 us -> 8.41 us  [over(): return lax.all_to_all(tiles, axes, 0, 0, tiled=True).reshape(array.shape)]
    ppermute x3, waiting for transfers between devices: 0.99 us -> 0.01 us  [from_other_core(): return lax.ppermute(array, 'tp', [(0, 1), (1, 0)])]
    pallas_call x2 -> x1, Pallas kernels: 1.29 us -> 1.18 us  [layer(): kernel(project, [shape((ROWS, PIECE), bf16), shape((ROWS, 128), bf16), sh...]
  transfers between devices with their start and end apart: 6 -> 6, of which waited for: 3 -> 2; matrix products, arithmetic and copies ran while one was open for 0% -> 0% of each run, Pallas kernels for 6% -> 5%
where the time goes in v1:
time: 64 us; the launch traced here: 63.7 us
  blocking collectives  31.8 us (50%)
  starting transfers between devices  14.3 us (22%)
  waiting for transfers between devices  10 us (16%)
  Pallas kernels  6.69 us (10%)
  between operations  0.79 us (1%)
    all_to_all x3, blocking collectives, over(): return lax.all_to_all(tiles, axes, 0, 0, tiled=True).reshape(array.shape)  31.8 us
    all_to_all x1, waiting for transfers between devices, over(): return lax.all_to_all(tiles, axes, 0, 0, tiled=True).reshape(array.shape)  8.41 us
    all_to_all x1, starting transfers between devices, over(): return lax.all_to_all(tiles, axes, 0, 0, tiled=True).reshape(array.shape)  7.87 us
    ppermute x3, starting transfers between devices, from_other_core(): return lax.ppermute(array, 'tp', [(0, 1), (1, 0)])  3.85 us
    ppermute x2, starting transfers between devices, from_ring(): return lax.ppermute(array, 'kv_1', [(i, i ^ flip) for i in range(RING)])  2.6 us
    ppermute x2, waiting for transfers between devices, from_ring(): return lax.ppermute(array, 'kv_1', [(i, i ^ flip) for i in range(RING)])  1.6 us
    pallas_call x1, Pallas kernels, updated(): pl.pallas_call(update, out_shape=[shape(operands[0].shape, f32), shape((8...  1.56 us
    pallas_call x1, Pallas kernels, preloaded(): pl.pallas_call(preload, out_shape=[shape(x.shape, x.dtype) for x in array...  1.31 us
  transfers between devices with their start and end apart: 6, of which 2 were waited for; matrix products, arithmetic and copies ran while one was open for 0% of the time, Pallas kernels for 5%

profile of v1, /device:TPU:1, one launch (start us, length us, event | category | flops | bytes accessed | tf_op | source)
XLA Modules:
  0.0 63.7 jit_solution(5821160050662942121)
XLA Ops:
  0.7 1.5 %collective-permute-start.1 = (bf16[512,128]{1,0:T(8,128)(2,1)}, bf16[512,128]{1,0:T(8,128)(2,1)S(1)}, u32[]{:S(2)}, u32[]{:S(2)}) collective-permute-start(bf16[512,128]{1,0:T(8,128)(2,1)} %refs_9_.1), channel_id=1, source_target_pairs={{0,1},{1,0},{2,3},{3,2},{4,5},{5,4},{6,7},{7,6},{8,9},{9,8},{10,11... | collective-permute-start | bytes 393224 | tf_op jit(solution)/shard_map/ppermute | solution.py:371
  2.1 0.1 collective-permute-start
  2.2 1.3 %preload.1 = (bf16[64,128]{1,0:T(8,128)(2,1)S(1)}, bf16[1,128]{1,0:T(2,128)(2,1)S(1)}, bf16[1,128]{1,0:T(2,128)(2,1)S(1)}, bf16[128,512]{1,0:T(8,128)(2,1)S(1)},...) custom-call(bf16[64,128]{1,0:T(8,128)(2,1)} %bitcast.34, ...), custom_call_target="tpu_custom_call" | custom-call | tf_op jit(solution)/shard_map/preload/pallas_call | solution.py:254
  3.5 0.0 collective-permute-done.other_ref
  3.5 0.0 collective-permute-done.1.other_mix_ref
  3.6 1.2 %shard_map.167 = (bf16[128,2176]{1,0:T(8,128)(2,1)}, bf16[128,128]{1,0:T(8,128)(2,1)S(1)}, bf16[544,128]{1,0:T(8,128)(2,1)S(1)}) custom-call(bf16[64,128]{1,0:T(8,128)(2,1)S(1)} %get-tuple-element.25.own_ref, bf16[1,128]{1,0:T(2,128)(2,1)S(1)} %get-tuple-element.26.gain_ref, bf16[1,128]{1,0:T(2,128)(2,1)S(1)} %get-tuple-element.27.gain_mid_ref, ...), custom_call_target="tpu_custom_call" | custom-call | tf_op jit(solution)/shard_map/pallas_call | solution.py:417
  4.7 7.9 %all-to-all-start = ((bf16[16,8,2176]{2,1,0:T(8,128)(2,1)}), bf16[16,8,2176]{2,1,0:T(8,128)(2,1)S(1)}, u32[]{:S(2)}, u32[]{:S(2)}) async-start(bf16[16,8,2176]{2,1,0:T(8,128)(2,1)} %bitcast.5), calls=%async_computation | async-start | bytes 1114112 | tf_op jit(solution)/shard_map/all_to_all | solution.py:376
  12.6 2.6 %collective-permute-start.2 = (bf16[544,128]{1,0:T(8,128)(2,1)S(1)}, bf16[544,128]{1,0:T(8,128)(2,1)S(1)}, u32[]{:S(2)}, u32[]{:S(2)}) collective-permute-start(bf16[544,128]{1,0:T(8,128)(2,1)S(1)} %get-tuple-element.37.held_ref), channel_id=1, source_target_pairs={{0,6},{2,4},{4,2},{6,0},{1,7},{3,5},{5,3},{7,1},{8,14},{10,12},{12... | collective-permute-start | bytes 417800 | tf_op jit(solution)/shard_map/ppermute | solution.py:380
  15.2 8.4 %all-to-all-done = bf16[16,8,2176]{2,1,0:T(8,128)(2,1)S(1)} async-done(((bf16[16,8,2176]{2,1,0:T(8,128)(2,1)}), bf16[16,8,2176]{2,1,0:T(8,128)(2,1)S(1)}, u32[]{:S(2)}, u32[]{:S(2)}) %all-to-all-start) | async-done | bytes 557088 | tf_op jit(solution)/shard_map/all_to_all | solution.py:376
  23.6 1.6 %collective-permute-done.2.near_ref = bf16[544,128]{1,0:T(8,128)(2,1)S(1)} collective-permute-done((bf16[544,128]{1,0:T(8,128)(2,1)S(1)}, bf16[544,128]{1,0:T(8,128)(2,1)S(1)}, u32[]{:S(2)}, u32[]{:S(2)}) %collective-permute-start.2) | collective-permute-done | bytes 139296 | tf_op jit(solution)/shard_map/ppermute | solution.py:380
  25.2 0.1 shard_map.170.joined_ref
  25.3 0.0 collective-permute-start.3
  25.4 0.0 copy-start.1
  25.4 0.0 copy-start.2
  25.4 0.5 shard_map.168
  25.9 9.9 %all_to_all.20 = bf16[8,8,512]{2,1,0:T(8,128)(2,1)S(1)} all-to-all(bf16[8,8,512]{2,1,0:T(8,128)(2,1)S(1)} %bitcast.29), channel_id=1, replica_groups=mesh['dp'=4,'kv_0'=4,'kv_1'=4,'tp'=2] {'kv_0','tp'}, dimensions={0} | all-to-all | bytes 131072 | tf_op jit(solution)/shard_map/all_to_all | solution.py:376
  35.8 0.4 shard_map.172
  36.2 10.8 %all_to_all.21 = bf16[16,32,256]{2,1,0:T(8,128)(2,1)S(1)} all-to-all(bf16[16,32,256]{2,1,0:T(8,128)(2,1)S(1)} %bitcast.23), channel_id=1, replica_groups=mesh['dp'=4,'kv_0'=4,'kv_1'=4,'tp'=2] {'kv_0','kv_1'}, dimensions={0} | all-to-all | bytes 524288 | tf_op jit(solution)/shard_map/all_to_all | solution.py:376
  47.0 0.5 gate_up.1
  47.6 2.3 %collective-permute-start.4 = (bf16[712,128]{1,0:T(8,128)(2,1)S(1)}, bf16[712,128]{1,0:T(8,128)(2,1)S(1)}, u32[]{:S(2)}, u32[]{:S(2)}) collective-permute-start(bf16[712,128]{1,0:T(8,128)(2,1)S(1)} %get-tuple-element.41), channel_id=1, source_target_pairs={{0,1},{1,0},{2,3},{3,2},{4,5},{5,4},{6,7},{7,6},{8,9},{9,8},{10,11... | collective-permute-start | bytes 546824 | tf_op jit(solution)/shard_map/ppermute | solution.py:371
  49.9 1.6 %update.1 = (f32[8,4,128,128]{3,2,1,0:T(8,128)}, f32[8,128]{1,0:T(8,128)S(1)}) custom-call(f32[8,4,128,128]{3,2,1,0:T(8,128)S(1)} %copy-done, f32[8,512]{1,0:T(8,128)S(1)} %get-tuple-element.42.key_ref, f32[8,512]{1,0:T(8,128)S(1)} %get-tuple-element.43.correct_ref, f32[8,128]{1,0:T(8,128)S(1)} %get-tuple-element.44.keep_ref, bf16[512,256]{1,0:T(8,128)(2,1)S(1)} %bitcast.21), custom_call_target="tpu_custom_call" | custom-call | tf_op jit(solution)/shard_map/update/pallas_call | solution.py:227
  51.5 0.5 shard_map.173
  51.9 11.1 %all_to_all.22 = bf16[16,64,128]{2,1,0:T(8,128)(2,1)S(1)} all-to-all(bf16[16,64,128]{2,1,0:T(8,128)(2,1)S(1)} %bitcast.24), channel_id=1, replica_groups=mesh['dp'=4,'kv_0'=4,'kv_1'=4,'tp'=2] {'kv_0','kv_1'}, dimensions={0} | all-to-all | bytes 524288 | tf_op jit(solution)/shard_map/all_to_all | solution.py:376
  63.0 0.6 %shard_map.174 = bf16[64,128]{1,0:T(8,128)(2,1)} custom-call(bf16[1024,128]{1,0:T(8,128)(2,1)S(1)} %bitcast.22, bf16[64,128]{1,0:T(8,128)(2,1)S(1)} %get-tuple-element.46.middle_ref), custom_call_target="tpu_custom_call" | custom-call | tf_op jit(solution)/shard_map/pallas_call | solution.py:463
  (14 shorter events, 0.0 us)
Async XLA Ops:
  0.6 24.7 %copy-start.4 = (f32[4]{0:T(128)S(1)}, f32[4]{0:T(128)}, u32[]{:S(2)}) copy-start(f32[4]{0:T(128)} %param.25) | copy-start | bytes 52
  0.6 24.7 %copy-start.5 = (f32[128]{0:T(128)S(1)}, f32[128]{0:T(128)}, u32[]{:S(2)}) copy-start(f32[128]{0:T(128)} %param.26) | copy-start | bytes 1540
  0.7 24.7 %copy-start = (f32[8,4,128,128]{3,2,1,0:T(8,128)S(1)}, f32[8,4,128,128]{3,2,1,0:T(8,128)}, u32[]{:S(2)}) copy-start(f32[8,4,128,128]{3,2,1,0:T(8,128)} %state_ref.3) | copy-start | bytes 6291460
  0.7 2.9 %collective-permute-start.1 = (bf16[512,128]{1,0:T(8,128)(2,1)}, bf16[512,128]{1,0:T(8,128)(2,1)S(1)}, u32[]{:S(2)}, u32[]{:S(2)}) collective-permute-start(bf16[512,128]{1,0:T(8,128)(2,1)} %refs_9_.1), channel_id=1, source_target_pairs={{0,1},{1,0},{2,3},{3,2},{4,5},{5,4},{6,7},{7,6},{8,9},{9,8},{10,11... | collective-permute-start | bytes 393224 | tf_op jit(solution)/shard_map/ppermute | solution.py:371
  2.1 1.4 %collective-permute-start = (bf16[64,128]{1,0:T(8,128)(2,1)}, bf16[64,128]{1,0:T(8,128)(2,1)S(1)}, u32[]{:S(2)}, u32[]{:S(2)}) collective-permute-start(bf16[64,128]{1,0:T(8,128)(2,1)} %bitcast.33), channel_id=1, source_target_pairs={{0,1},{1,0},{2,3},{3,2},{4,5},{5,4},{6,7},{7,6},{8,9},{9,8},{10,11... | collective-permute-start | bytes 49160 | tf_op jit(solution)/shard_map/ppermute | solution.py:371
  4.7 18.9 %all-to-all-start = ((bf16[16,8,2176]{2,1,0:T(8,128)(2,1)}), bf16[16,8,2176]{2,1,0:T(8,128)(2,1)S(1)}, u32[]{:S(2)}, u32[]{:S(2)}) async-start(bf16[16,8,2176]{2,1,0:T(8,128)(2,1)} %bitcast.5), calls=%async_computation | async-start | bytes 1114112 | tf_op jit(solution)/shard_map/all_to_all | solution.py:376
  12.6 12.6 %collective-permute-start.2 = (bf16[544,128]{1,0:T(8,128)(2,1)S(1)}, bf16[544,128]{1,0:T(8,128)(2,1)S(1)}, u32[]{:S(2)}, u32[]{:S(2)}) collective-permute-start(bf16[544,128]{1,0:T(8,128)(2,1)S(1)} %get-tuple-element.37.held_ref), channel_id=1, source_target_pairs={{0,6},{2,4},{4,2},{6,0},{1,7},{3,5},{5,3},{7,1},{8,14},{10,12},{12... | collective-permute-start | bytes 417800 | tf_op jit(solution)/shard_map/ppermute | solution.py:380
  25.3 10.5 %collective-permute-start.3 = (bf16[1056,128]{1,0:T(8,128)(2,1)S(1)}, bf16[1056,128]{1,0:T(8,128)(2,1)S(1)}, u32[]{:S(2)}, u32[]{:S(2)}) collective-permute-start(bf16[1056,128]{1,0:T(8,128)(2,1)S(1)} %shard_map.170.joined_ref), channel_id=1, source_target_pairs={{0,2},{2,0},{4,6},{6,4},{1,3},{3,1},{5,7},{7,5},{8,10},{10,8},{12,... | collective-permute-start | bytes 811016 | tf_op jit(solution)/shard_map/ppermute | solution.py:380
  25.4 21.7 %copy-start.1 = (bf16[1024,352]{0,1:T(8,128)(2,1)S(1)}, bf16[1024,352]{0,1:T(8,128)(2,1)}, u32[]{:S(2)}) copy-start(bf16[1024,352]{0,1:T(8,128)(2,1)} %param.29) | copy-start | bytes 2162692
  25.4 21.6 %copy-start.2 = (bf16[1024,352]{0,1:T(8,128)(2,1)S(1)}, bf16[1024,352]{0,1:T(8,128)(2,1)}, u32[]{:S(2)}) copy-start(bf16[1024,352]{0,1:T(8,128)(2,1)} %param.30) | copy-start | bytes 2162692
  47.0 4.4 %copy-start.3 = (bf16[352,1024]{1,0:T(8,128)(2,1)S(1)}, bf16[352,1024]{1,0:T(8,128)(2,1)}, u32[]{:S(2)}) copy-start(bf16[352,1024]{1,0:T(8,128)(2,1)} %w_ref.1) | copy-start | bytes 2162692
  47.6 3.9 %collective-permute-start.4 = (bf16[712,128]{1,0:T(8,128)(2,1)S(1)}, bf16[712,128]{1,0:T(8,128)(2,1)S(1)}, u32[]{:S(2)}, u32[]{:S(2)}) collective-permute-start(bf16[712,128]{1,0:T(8,128)(2,1)S(1)} %get-tuple-element.41), channel_id=1, source_target_pairs={{0,1},{1,0},{2,3},{3,2},{4,5},{5,4},{6,7},{7,6},{8,9},{9,8},{10,11... | collective-permute-start | bytes 546824 | tf_op jit(solution)/shard_map/ppermute | solution.py:371

commit v2 on v1

--- a/solution.py
+++ b/solution.py
@@ -279,14 +279,7 @@
 
 
 def ring_parts(received_ref, joined_ref):
-    mixed = jnp.concatenate(
-        [
-            received_ref[OWN * (2 * r + core) : OWN * (2 * r + core + 1)].astype(f32)
-            for core in range(2)
-            for r in range(RING)
-        ],
-        axis=0,
-    ).astype(bf16)
+    mixed = received_ref[...]
     parts = []
     for at in (0, WIDTH_DEV):
         both = dot(mixed, joined_ref[at : at + WIDTH_DEV])
@@ -437,7 +430,7 @@
         ],
         [v] * 4,
     )(pieces, delta_state, decay_rate.reshape(1, HEADS_DEV), head_gain.reshape(1, HEAD_DIM))
-    mixed_rows = over(mixed, ("kv_0", "tp"), 2 * RING)
+    mixed_rows = over(mixed, ("tp", "kv_0"), 2 * RING)
     arrived = kernel(note, shape((8, 128), f32), [a])(mixed_rows)
     sent = kernel(mix, shape((GROUP * SEQ_RING, FEAT_RING), bf16), [v] * 5 + [a])(
         mixed_rows, joined, near, far, rows, arrived

time: 64 us -> 64 us (level)
  no operation moved by 1% of the time
where the time goes in v2:
time: 64 us; the launch traced here: 63.7 us
  blocking collectives  32 us (50%)
  starting transfers between devices  14.2 us (22%)
  waiting for transfers between devices  10 us (16%)
  Pallas kernels  6.69 us (10%)
  between operations  0.79 us (1%)
    all_to_all x3, blocking collectives, over(): return lax.all_to_all(tiles, axes, 0, 0, tiled=True).reshape(array.shape)  32 us
    all_to_all x1, waiting for transfers between devices, over(): return lax.all_to_all(tiles, axes, 0, 0, tiled=True).reshape(array.shape)  8.41 us
    all_to_all x1, starting transfers between devices, over(): return lax.all_to_all(tiles, axes, 0, 0, tiled=True).reshape(array.shape)  7.87 us
    ppermute x3, starting transfers between devices, from_other_core(): return lax.ppermute(array, 'tp', [(0, 1), (1, 0)])  3.71 us
    ppermute x2, starting transfers between devices, from_ring(): return lax.ppermute(array, 'kv_1', [(i, i ^ flip) for i in range(RING)])  2.6 us
    ppermute x2, waiting for transfers between devices, from_ring(): return lax.ppermute(array, 'kv_1', [(i, i ^ flip) for i in range(RING)])  1.6 us
    pallas_call x1, Pallas kernels, updated(): pl.pallas_call(update, out_shape=[shape(operands[0].shape, f32), shape((8...  1.56 us
    pallas_call x1, Pallas kernels, preloaded(): pl.pallas_call(preload, out_shape=[shape(x.shape, x.dtype) for x in array...  1.31 us
  transfers between devices with their start and end apart: 6, of which 2 were waited for; matrix products, arithmetic and copies ran while one was open for 0% of the time, Pallas kernels for 5%

profile of v2, /device:TPU:1, one launch (start us, length us, event | category | flops | bytes accessed | tf_op | source)
XLA Modules:
  0.0 63.7 jit_solution(18210868516579960778)
XLA Ops:
  0.7 1.5 %collective-permute-start.1 = (bf16[512,128]{1,0:T(8,128)(2,1)}, bf16[512,128]{1,0:T(8,128)(2,1)S(1)}, u32[]{:S(2)}, u32[]{:S(2)}) collective-permute-start(bf16[512,128]{1,0:T(8,128)(2,1)} %refs_9_.1), channel_id=1, source_target_pairs={{0,1},{1,0},{2,3},{3,2},{4,5},{5,4},{6,7},{7,6},{8,9},{9,8},{10,11... | collective-permute-start | bytes 393224 | tf_op jit(solution)/shard_map/ppermute | solution.py:364
  2.1 0.1 collective-permute-start
  2.2 1.3 %preload.1 = (bf16[64,128]{1,0:T(8,128)(2,1)S(1)}, bf16[1,128]{1,0:T(2,128)(2,1)S(1)}, bf16[1,128]{1,0:T(2,128)(2,1)S(1)}, bf16[128,512]{1,0:T(8,128)(2,1)S(1)},...) custom-call(bf16[64,128]{1,0:T(8,128)(2,1)} %bitcast.34, ...), custom_call_target="tpu_custom_call" | custom-call | tf_op jit(solution)/shard_map/preload/pallas_call | solution.py:254
  3.5 0.0 collective-permute-done.other_ref
  3.5 0.0 collective-permute-done.1.other_mix_ref
  3.6 1.2 %shard_map.167 = (bf16[128,2176]{1,0:T(8,128)(2,1)}, bf16[128,128]{1,0:T(8,128)(2,1)S(1)}, bf16[544,128]{1,0:T(8,128)(2,1)S(1)}) custom-call(bf16[64,128]{1,0:T(8,128)(2,1)S(1)} %get-tuple-element.25.own_ref, bf16[1,128]{1,0:T(2,128)(2,1)S(1)} %get-tuple-element.26.gain_ref, bf16[1,128]{1,0:T(2,128)(2,1)S(1)} %get-tuple-element.27.gain_mid_ref, ...), custom_call_target="tpu_custom_call" | custom-call | tf_op jit(solution)/shard_map/pallas_call | solution.py:410
  4.7 7.9 %all-to-all-start = ((bf16[16,8,2176]{2,1,0:T(8,128)(2,1)}), bf16[16,8,2176]{2,1,0:T(8,128)(2,1)S(1)}, u32[]{:S(2)}, u32[]{:S(2)}) async-start(bf16[16,8,2176]{2,1,0:T(8,128)(2,1)} %bitcast.5), calls=%async_computation | async-start | bytes 1114112 | tf_op jit(solution)/shard_map/all_to_all | solution.py:369
  12.6 2.6 %collective-permute-start.2 = (bf16[544,128]{1,0:T(8,128)(2,1)S(1)}, bf16[544,128]{1,0:T(8,128)(2,1)S(1)}, u32[]{:S(2)}, u32[]{:S(2)}) collective-permute-start(bf16[544,128]{1,0:T(8,128)(2,1)S(1)} %get-tuple-element.37.held_ref), channel_id=1, source_target_pairs={{0,6},{2,4},{4,2},{6,0},{1,7},{3,5},{5,3},{7,1},{8,14},{10,12},{12... | collective-permute-start | bytes 417800 | tf_op jit(solution)/shard_map/ppermute | solution.py:373
  15.2 8.4 %all-to-all-done = bf16[16,8,2176]{2,1,0:T(8,128)(2,1)S(1)} async-done(((bf16[16,8,2176]{2,1,0:T(8,128)(2,1)}), bf16[16,8,2176]{2,1,0:T(8,128)(2,1)S(1)}, u32[]{:S(2)}, u32[]{:S(2)}) %all-to-all-start) | async-done | bytes 557088 | tf_op jit(solution)/shard_map/all_to_all | solution.py:369
  23.6 1.6 %collective-permute-done.2.near_ref = bf16[544,128]{1,0:T(8,128)(2,1)S(1)} collective-permute-done((bf16[544,128]{1,0:T(8,128)(2,1)S(1)}, bf16[544,128]{1,0:T(8,128)(2,1)S(1)}, u32[]{:S(2)}, u32[]{:S(2)}) %collective-permute-start.2) | collective-permute-done | bytes 139296 | tf_op jit(solution)/shard_map/ppermute | solution.py:373
  25.2 0.1 shard_map.170.joined_ref
  25.3 0.0 collective-permute-start.3
  25.4 0.0 copy-start.1
  25.4 0.0 copy-start.2
  25.4 0.5 shard_map.168
  25.9 10.0 %all_to_all.20 = bf16[8,8,512]{2,1,0:T(8,128)(2,1)S(1)} all-to-all(bf16[8,8,512]{2,1,0:T(8,128)(2,1)S(1)} %bitcast.29), channel_id=1, replica_groups=mesh['dp'=4,'kv_0'=4,'kv_1'=4,'tp'=2] {'tp','kv_0'}, dimensions={0} | all-to-all | bytes 131072 | tf_op jit(solution)/shard_map/all_to_all | solution.py:369
  35.9 0.4 shard_map.172
  36.3 10.8 %all_to_all.21 = bf16[16,32,256]{2,1,0:T(8,128)(2,1)S(1)} all-to-all(bf16[16,32,256]{2,1,0:T(8,128)(2,1)S(1)} %bitcast.23), channel_id=1, replica_groups=mesh['dp'=4,'kv_0'=4,'kv_1'=4,'tp'=2] {'kv_0','kv_1'}, dimensions={0} | all-to-all | bytes 524288 | tf_op jit(solution)/shard_map/all_to_all | solution.py:369
  47.2 0.6 gate_up.1
  47.7 2.2 %collective-permute-start.4 = (bf16[712,128]{1,0:T(8,128)(2,1)S(1)}, bf16[712,128]{1,0:T(8,128)(2,1)S(1)}, u32[]{:S(2)}, u32[]{:S(2)}) collective-permute-start(bf16[712,128]{1,0:T(8,128)(2,1)S(1)} %get-tuple-element.41), channel_id=1, source_target_pairs={{0,1},{1,0},{2,3},{3,2},{4,5},{5,4},{6,7},{7,6},{8,9},{9,8},{10,11... | collective-permute-start | bytes 546824 | tf_op jit(solution)/shard_map/ppermute | solution.py:364
  49.9 1.6 %update.1 = (f32[8,4,128,128]{3,2,1,0:T(8,128)}, f32[8,128]{1,0:T(8,128)S(1)}) custom-call(f32[8,4,128,128]{3,2,1,0:T(8,128)S(1)} %copy-done, f32[8,512]{1,0:T(8,128)S(1)} %get-tuple-element.42.key_ref, f32[8,512]{1,0:T(8,128)S(1)} %get-tuple-element.43.correct_ref, f32[8,128]{1,0:T(8,128)S(1)} %get-tuple-element.44.keep_ref, bf16[512,256]{1,0:T(8,128)(2,1)S(1)} %bitcast.21), custom_call_target="tpu_custom_call" | custom-call | tf_op jit(solution)/shard_map/update/pallas_call | solution.py:227
  51.5 0.5 shard_map.173
  51.9 11.1 %all_to_all.22 = bf16[16,64,128]{2,1,0:T(8,128)(2,1)S(1)} all-to-all(bf16[16,64,128]{2,1,0:T(8,128)(2,1)S(1)} %bitcast.24), channel_id=1, replica_groups=mesh['dp'=4,'kv_0'=4,'kv_1'=4,'tp'=2] {'kv_0','kv_1'}, dimensions={0} | all-to-all | bytes 524288 | tf_op jit(solution)/shard_map/all_to_all | solution.py:369
  63.0 0.6 %shard_map.174 = bf16[64,128]{1,0:T(8,128)(2,1)} custom-call(bf16[1024,128]{1,0:T(8,128)(2,1)S(1)} %bitcast.22, bf16[64,128]{1,0:T(8,128)(2,1)S(1)} %get-tuple-element.46.middle_ref), custom_call_target="tpu_custom_call" | custom-call | tf_op jit(solution)/shard_map/pallas_call | solution.py:456
  (14 shorter events, 0.0 us)
Async XLA Ops:
  0.6 24.7 %copy-start.4 = (f32[4]{0:T(128)S(1)}, f32[4]{0:T(128)}, u32[]{:S(2)}) copy-start(f32[4]{0:T(128)} %param.25) | copy-start | bytes 52
  0.6 24.7 %copy-start.5 = (f32[128]{0:T(128)S(1)}, f32[128]{0:T(128)}, u32[]{:S(2)}) copy-start(f32[128]{0:T(128)} %param.26) | copy-start | bytes 1540
  0.7 24.7 %copy-start = (f32[8,4,128,128]{3,2,1,0:T(8,128)S(1)}, f32[8,4,128,128]{3,2,1,0:T(8,128)}, u32[]{:S(2)}) copy-start(f32[8,4,128,128]{3,2,1,0:T(8,128)} %state_ref.3) | copy-start | bytes 6291460
  0.7 2.9 %collective-permute-start.1 = (bf16[512,128]{1,0:T(8,128)(2,1)}, bf16[512,128]{1,0:T(8,128)(2,1)S(1)}, u32[]{:S(2)}, u32[]{:S(2)}) collective-permute-start(bf16[512,128]{1,0:T(8,128)(2,1)} %refs_9_.1), channel_id=1, source_target_pairs={{0,1},{1,0},{2,3},{3,2},{4,5},{5,4},{6,7},{7,6},{8,9},{9,8},{10,11... | collective-permute-start | bytes 393224 | tf_op jit(solution)/shard_map/ppermute | solution.py:364
  2.1 1.4 %collective-permute-start = (bf16[64,128]{1,0:T(8,128)(2,1)}, bf16[64,128]{1,0:T(8,128)(2,1)S(1)}, u32[]{:S(2)}, u32[]{:S(2)}) collective-permute-start(bf16[64,128]{1,0:T(8,128)(2,1)} %bitcast.33), channel_id=1, source_target_pairs={{0,1},{1,0},{2,3},{3,2},{4,5},{5,4},{6,7},{7,6},{8,9},{9,8},{10,11... | collective-permute-start | bytes 49160 | tf_op jit(solution)/shard_map/ppermute | solution.py:364
  4.7 18.9 %all-to-all-start = ((bf16[16,8,2176]{2,1,0:T(8,128)(2,1)}), bf16[16,8,2176]{2,1,0:T(8,128)(2,1)S(1)}, u32[]{:S(2)}, u32[]{:S(2)}) async-start(bf16[16,8,2176]{2,1,0:T(8,128)(2,1)} %bitcast.5), calls=%async_computation | async-start | bytes 1114112 | tf_op jit(solution)/shard_map/all_to_all | solution.py:369
  12.6 12.6 %collective-permute-start.2 = (bf16[544,128]{1,0:T(8,128)(2,1)S(1)}, bf16[544,128]{1,0:T(8,128)(2,1)S(1)}, u32[]{:S(2)}, u32[]{:S(2)}) collective-permute-start(bf16[544,128]{1,0:T(8,128)(2,1)S(1)} %get-tuple-element.37.held_ref), channel_id=1, source_target_pairs={{0,6},{2,4},{4,2},{6,0},{1,7},{3,5},{5,3},{7,1},{8,14},{10,12},{12... | collective-permute-start | bytes 417800 | tf_op jit(solution)/shard_map/ppermute | solution.py:373
  25.3 10.6 %collective-permute-start.3 = (bf16[1056,128]{1,0:T(8,128)(2,1)S(1)}, bf16[1056,128]{1,0:T(8,128)(2,1)S(1)}, u32[]{:S(2)}, u32[]{:S(2)}) collective-permute-start(bf16[1056,128]{1,0:T(8,128)(2,1)S(1)} %shard_map.170.joined_ref), channel_id=1, source_target_pairs={{0,2},{2,0},{4,6},{6,4},{1,3},{3,1},{5,7},{7,5},{8,10},{10,8},{12,... | collective-permute-start | bytes 811016 | tf_op jit(solution)/shard_map/ppermute | solution.py:373
  25.4 21.8 %copy-start.1 = (bf16[1024,352]{0,1:T(8,128)(2,1)S(1)}, bf16[1024,352]{0,1:T(8,128)(2,1)}, u32[]{:S(2)}) copy-start(bf16[1024,352]{0,1:T(8,128)(2,1)} %param.29) | copy-start | bytes 2162692
  25.4 21.8 %copy-start.2 = (bf16[1024,352]{0,1:T(8,128)(2,1)S(1)}, bf16[1024,352]{0,1:T(8,128)(2,1)}, u32[]{:S(2)}) copy-start(bf16[1024,352]{0,1:T(8,128)(2,1)} %param.30) | copy-start | bytes 2162692
  47.1 4.3 %copy-start.3 = (bf16[352,1024]{1,0:T(8,128)(2,1)S(1)}, bf16[352,1024]{1,0:T(8,128)(2,1)}, u32[]{:S(2)}) copy-start(bf16[352,1024]{1,0:T(8,128)(2,1)} %w_ref.1) | copy-start | bytes 2162692
  47.7 3.7 %collective-permute-start.4 = (bf16[712,128]{1,0:T(8,128)(2,1)S(1)}, bf16[712,128]{1,0:T(8,128)(2,1)S(1)}, u32[]{:S(2)}, u32[]{:S(2)}) collective-permute-start(bf16[712,128]{1,0:T(8,128)(2,1)S(1)} %get-tuple-element.41), channel_id=1, source_target_pairs={{0,1},{1,0},{2,3},{3,2},{4,5},{5,4},{6,7},{7,6},{8,9},{9,8},{10,11... | collective-permute-start | bytes 546824 | tf_op jit(solution)/shard_map/ppermute | solution.py:364

commit v3 on v2

--- a/solution.py
+++ b/solution.py
@@ -78,7 +78,7 @@
 
 
 def project(
-    own_ref, gain_ref, gain_mid_ref, wq_ref, wk_ref, wv_ref, wg_ref, wb_ref, wd_ref, own_mix_ref, other_ref, other_mix_ref, out_ref, rows_ref, held_ref
+    own_ref, gain_ref, gain_mid_ref, wq_ref, wk_ref, wv_ref, wg_ref, wb_ref, wd_ref, own_mix_ref, other_ref, other_mix_ref, out_ref, rows_ref, held_ref, joined_ref
 ):
     on_first = lax.axis_index("tp") == 0
     own = own_ref[...].astype(f32)
@@ -109,6 +109,9 @@
     extra = jnp.where(lane == 2 * HEADS_DEV + 1, low, extra)
     out_ref[:, SMALL_AT:] = jnp.where(lane >= 64, gain_mid, extra).astype(bf16)
     pack(own_mix_ref, other_mix_ref, rows_ref, held_ref)
+    joined_ref[:WIDTH_DEV] = held_ref[:WIDTH_DEV]
+    near_place = jnp.bitwise_xor(lax.axis_index("kv_1"), 1)
+    joined_ref[2 * WIDTH_DEV :] = ring_tokens(rows_ref, near_place, on_first, True).astype(bf16)
 
 
 def low_lanes(value):
@@ -267,14 +270,11 @@
     out_ref[...] = jnp.zeros(out_ref.shape, f32)
 
 
-def join(held_ref, near_ref, rows_ref, after_ref, out_ref):
+def join(base_ref, near_ref, after_ref, out_ref):
     del after_ref
-    on_first = lax.axis_index("tp") == 0
-    place = lax.axis_index("kv_1")
-    out_ref[:WIDTH_DEV] = held_ref[:WIDTH_DEV]
+    first = base_ref[2 * WIDTH_DEV :].astype(f32)
+    second = near_ref[WIDTH_DEV:].astype(f32)
     out_ref[WIDTH_DEV : 2 * WIDTH_DEV] = near_ref[:WIDTH_DEV]
-    first = ring_tokens(rows_ref, jnp.bitwise_xor(place, 1), on_first, True)
-    second = near_ref[WIDTH_DEV:].astype(f32)
     out_ref[2 * WIDTH_DEV :] = jnp.where(low_lanes(first), first, second).astype(bf16)
 
 
@@ -407,17 +407,28 @@
         w_decay.T,
         w_mix,
     )
-    summand, rows, held = kernel(
+    summand, rows, held, base = kernel(
         project,
-        [shape((ROWS, PIECE), bf16), shape((ROWS, 128), bf16), shape((PACKED, 128), bf16)],
+        [
+            shape((ROWS, PIECE), bf16),
+            shape((ROWS, 128), bf16),
+            shape((PACKED, 128), bf16),
+            shape((JOINED, 128), bf16),
+        ],
         [v] * 12,
     )(*loaded, other_tokens, other_mix)
     near = from_ring(held, 3)
     pieces = over(summand, KV, GROUP)
     mark = kernel(note, shape((8, 128), f32), [a])(pieces)
-    joined = kernel(join, shape((JOINED, 128), bf16), [v] * 3 + [a])(
-        held, near, rows, mark
-    )
+    joined = pl.pallas_call(
+        join,
+        out_shape=shape((JOINED, 128), bf16),
+        in_specs=[v, v, anywhere()],
+        out_specs=v,
+        input_output_aliases={0: 0},
+        name="join",
+        compiler_params=pltpu.CompilerParams(vmem_limit_bytes=12 * 1024 * 1024),
+    )(base, near, mark)
     far = from_ring(joined, 1)
     mixed, key, correction, keep, gains = kernel(
         mixer,

time: 64 us -> 64 us (level)
  no operation moved by 1% of the time
where the time goes in v3:
time: 64 us; the launch traced here: 63.7 us
  blocking collectives  32 us (50%)
  starting transfers between devices  14.3 us (22%)
  waiting for transfers between devices  10 us (16%)
  Pallas kernels  6.63 us (10%)
  between operations  0.8 us (1%)
    all_to_all x3, blocking collectives, over(): return lax.all_to_all(tiles, axes, 0, 0, tiled=True).reshape(array.shape)  32 us
    all_to_all x1, waiting for transfers between devices, over(): return lax.all_to_all(tiles, axes, 0, 0, tiled=True).reshape(array.shape)  8.43 us
    all_to_all x1, starting transfers between devices, over(): return lax.all_to_all(tiles, axes, 0, 0, tiled=True).reshape(array.shape)  7.88 us
    ppermute x3, starting transfers between devices, from_other_core(): return lax.ppermute(array, 'tp', [(0, 1), (1, 0)])  3.72 us
    ppermute x2, starting transfers between devices, from_ring(): return lax.ppermute(array, 'kv_1', [(i, i ^ flip) for i in range(RING)])  2.66 us
    ppermute x2, waiting for transfers between devices, from_ring(): return lax.ppermute(array, 'kv_1', [(i, i ^ flip) for i in range(RING)])  1.59 us
    pallas_call x1, Pallas kernels, updated(): pl.pallas_call(update, out_shape=[shape(operands[0].shape, f32), shape((8...  1.56 us
    pallas_call x1, Pallas kernels, preloaded(): pl.pallas_call(preload, out_shape=[shape(x.shape, x.dtype) for x in array...  1.31 us
  transfers between devices with their start and end apart: 6, of which 2 were waited for; matrix products, arithmetic and copies ran while one was open for 0% of the time, Pallas kernels for 5%

profile of v3, /device:TPU:1, one launch (start us, length us, event | category | flops | bytes accessed | tf_op | source)
XLA Modules:
  0.0 63.7 jit_solution(8516108315322003146)
XLA Ops:
  0.7 1.5 %collective-permute-start.1 = (bf16[512,128]{1,0:T(8,128)(2,1)}, bf16[512,128]{1,0:T(8,128)(2,1)S(1)}, u32[]{:S(2)}, u32[]{:S(2)}) collective-permute-start(bf16[512,128]{1,0:T(8,128)(2,1)} %refs_9_.1), channel_id=1, source_target_pairs={{0,1},{1,0},{2,3},{3,2},{4,5},{5,4},{6,7},{7,6},{8,9},{9,8},{10,11... | collective-permute-start | bytes 393224 | tf_op jit(solution)/shard_map/ppermute | solution.py:364
  2.1 0.1 collective-permute-start
  2.2 1.3 %preload.1 = (bf16[64,128]{1,0:T(8,128)(2,1)S(1)}, bf16[1,128]{1,0:T(2,128)(2,1)S(1)}, bf16[1,128]{1,0:T(2,128)(2,1)S(1)}, bf16[128,512]{1,0:T(8,128)(2,1)S(1)},...) custom-call(bf16[64,128]{1,0:T(8,128)(2,1)} %bitcast.34, ...), custom_call_target="tpu_custom_call" | custom-call | tf_op jit(solution)/shard_map/preload/pallas_call | solution.py:257
  3.5 0.0 collective-permute-done.other_ref
  3.5 0.0 collective-permute-done.1.other_mix_ref
  3.6 1.2 %shard_map.167 = (bf16[128,2176]{1,0:T(8,128)(2,1)}, bf16[128,128]{1,0:T(8,128)(2,1)S(1)}, bf16[544,128]{1,0:T(8,128)(2,1)S(1)}, bf16[1056,128]{1,0:T(8,128)(2,1)S(1)}) custom-call(bf16[64,128]{1,0:T(8,128)(2,1)S(1)} %get-tuple-element.26.own_ref, bf16[1,128]{1,0:T(2,128)(2,1)S(1)} %get-tuple-element.27.gain_ref, ...), custom_call_target="tpu_custom_call" | custom-call | tf_op jit(solution)/shard_map/pallas_call | solution.py:410
  4.8 7.9 %all-to-all-start = ((bf16[16,8,2176]{2,1,0:T(8,128)(2,1)}), bf16[16,8,2176]{2,1,0:T(8,128)(2,1)S(1)}, u32[]{:S(2)}, u32[]{:S(2)}) async-start(bf16[16,8,2176]{2,1,0:T(8,128)(2,1)} %bitcast.5), calls=%async_computation | async-start | bytes 1114112 | tf_op jit(solution)/shard_map/all_to_all | solution.py:369
  12.6 2.6 %collective-permute-start.2 = (bf16[544,128]{1,0:T(8,128)(2,1)S(1)}, bf16[544,128]{1,0:T(8,128)(2,1)S(1)}, u32[]{:S(2)}, u32[]{:S(2)}) collective-permute-start(bf16[544,128]{1,0:T(8,128)(2,1)S(1)} %get-tuple-element.39), channel_id=1, source_target_pairs={{0,6},{2,4},{4,2},{6,0},{1,7},{3,5},{5,3},{7,1},{8,14},{10,12},{12... | collective-permute-start | bytes 417800 | tf_op jit(solution)/shard_map/ppermute | solution.py:373
  15.2 8.4 %all-to-all-done = bf16[16,8,2176]{2,1,0:T(8,128)(2,1)S(1)} async-done(((bf16[16,8,2176]{2,1,0:T(8,128)(2,1)}), bf16[16,8,2176]{2,1,0:T(8,128)(2,1)S(1)}, u32[]{:S(2)}, u32[]{:S(2)}) %all-to-all-start) | async-done | bytes 557088 | tf_op jit(solution)/shard_map/all_to_all | solution.py:369
  23.7 1.6 %collective-permute-done.2.near_ref = bf16[544,128]{1,0:T(8,128)(2,1)S(1)} collective-permute-done((bf16[544,128]{1,0:T(8,128)(2,1)S(1)}, bf16[544,128]{1,0:T(8,128)(2,1)S(1)}, u32[]{:S(2)}, u32[]{:S(2)}) %collective-permute-start.2) | collective-permute-done | bytes 139296 | tf_op jit(solution)/shard_map/ppermute | solution.py:373
  25.3 0.1 collective-permute-start.3
  25.4 0.0 copy-start.1
  25.4 0.0 copy-start.2
  25.4 0.5 shard_map.168
  25.9 10.0 %all_to_all.20 = bf16[8,8,512]{2,1,0:T(8,128)(2,1)S(1)} all-to-all(bf16[8,8,512]{2,1,0:T(8,128)(2,1)S(1)} %bitcast.29), channel_id=1, replica_groups=mesh['dp'=4,'kv_0'=4,'kv_1'=4,'tp'=2] {'tp','kv_0'}, dimensions={0} | all-to-all | bytes 131072 | tf_op jit(solution)/shard_map/all_to_all | solution.py:369
  35.9 0.0 collective-permute-done.3.far_ref
  35.9 0.4 shard_map.171
  36.3 10.8 %all_to_all.21 = bf16[16,32,256]{2,1,0:T(8,128)(2,1)S(1)} all-to-all(bf16[16,32,256]{2,1,0:T(8,128)(2,1)S(1)} %bitcast.23), channel_id=1, replica_groups=mesh['dp'=4,'kv_0'=4,'kv_1'=4,'tp'=2] {'kv_0','kv_1'}, dimensions={0} | all-to-all | bytes 524288 | tf_op jit(solution)/shard_map/all_to_all | solution.py:369
  47.2 0.6 gate_up.1
  47.7 2.2 %collective-permute-start.4 = (bf16[712,128]{1,0:T(8,128)(2,1)S(1)}, bf16[712,128]{1,0:T(8,128)(2,1)S(1)}, u32[]{:S(2)}, u32[]{:S(2)}) collective-permute-start(bf16[712,128]{1,0:T(8,128)(2,1)S(1)} %get-tuple-element.43), channel_id=1, source_target_pairs={{0,1},{1,0},{2,3},{3,2},{4,5},{5,4},{6,7},{7,6},{8,9},{9,8},{10,11... | collective-permute-start | bytes 546824 | tf_op jit(solution)/shard_map/ppermute | solution.py:364
  49.9 1.6 %update.1 = (f32[8,4,128,128]{3,2,1,0:T(8,128)}, f32[8,128]{1,0:T(8,128)S(1)}) custom-call(f32[8,4,128,128]{3,2,1,0:T(8,128)S(1)} %copy-done, f32[8,512]{1,0:T(8,128)S(1)} %get-tuple-element.44.key_ref, f32[8,512]{1,0:T(8,128)S(1)} %get-tuple-element.45.correct_ref, f32[8,128]{1,0:T(8,128)S(1)} %get-tuple-element.46.keep_ref, bf16[512,256]{1,0:T(8,128)(2,1)S(1)} %bitcast.21), custom_call_target="tpu_custom_call" | custom-call | tf_op jit(solution)/shard_map/update/pallas_call | solution.py:230
  51.5 0.4 shard_map.172
  51.9 11.1 %all_to_all.22 = bf16[16,64,128]{2,1,0:T(8,128)(2,1)S(1)} all-to-all(bf16[16,64,128]{2,1,0:T(8,128)(2,1)S(1)} %bitcast.24), channel_id=1, replica_groups=mesh['dp'=4,'kv_0'=4,'kv_1'=4,'tp'=2] {'kv_0','kv_1'}, dimensions={0} | all-to-all | bytes 524288 | tf_op jit(solution)/shard_map/all_to_all | solution.py:369
  63.0 0.6 %shard_map.173 = bf16[64,128]{1,0:T(8,128)(2,1)} custom-call(bf16[1024,128]{1,0:T(8,128)(2,1)S(1)} %bitcast.22, bf16[64,128]{1,0:T(8,128)(2,1)S(1)} %get-tuple-element.48.middle_ref), custom_call_target="tpu_custom_call" | custom-call | tf_op jit(solution)/shard_map/pallas_call | solution.py:467
  (14 shorter events, 0.0 us)
Async XLA Ops:
  0.6 24.7 %copy-start.4 = (f32[4]{0:T(128)S(1)}, f32[4]{0:T(128)}, u32[]{:S(2)}) copy-start(f32[4]{0:T(128)} %param.25) | copy-start | bytes 52
  0.6 24.7 %copy-start.5 = (f32[128]{0:T(128)S(1)}, f32[128]{0:T(128)}, u32[]{:S(2)}) copy-start(f32[128]{0:T(128)} %param.26) | copy-start | bytes 1540
  0.7 24.7 %copy-start = (f32[8,4,128,128]{3,2,1,0:T(8,128)S(1)}, f32[8,4,128,128]{3,2,1,0:T(8,128)}, u32[]{:S(2)}) copy-start(f32[8,4,128,128]{3,2,1,0:T(8,128)} %state_ref.3) | copy-start | bytes 6291460
  0.7 2.9 %collective-permute-start.1 = (bf16[512,128]{1,0:T(8,128)(2,1)}, bf16[512,128]{1,0:T(8,128)(2,1)S(1)}, u32[]{:S(2)}, u32[]{:S(2)}) collective-permute-start(bf16[512,128]{1,0:T(8,128)(2,1)} %refs_9_.1), channel_id=1, source_target_pairs={{0,1},{1,0},{2,3},{3,2},{4,5},{5,4},{6,7},{7,6},{8,9},{9,8},{10,11... | collective-permute-start | bytes 393224 | tf_op jit(solution)/shard_map/ppermute | solution.py:364
  2.1 1.4 %collective-permute-start = (bf16[64,128]{1,0:T(8,128)(2,1)}, bf16[64,128]{1,0:T(8,128)(2,1)S(1)}, u32[]{:S(2)}, u32[]{:S(2)}) collective-permute-start(bf16[64,128]{1,0:T(8,128)(2,1)} %bitcast.33), channel_id=1, source_target_pairs={{0,1},{1,0},{2,3},{3,2},{4,5},{5,4},{6,7},{7,6},{8,9},{9,8},{10,11... | collective-permute-start | bytes 49160 | tf_op jit(solution)/shard_map/ppermute | solution.py:364
  4.8 18.9 %all-to-all-start = ((bf16[16,8,2176]{2,1,0:T(8,128)(2,1)}), bf16[16,8,2176]{2,1,0:T(8,128)(2,1)S(1)}, u32[]{:S(2)}, u32[]{:S(2)}) async-start(bf16[16,8,2176]{2,1,0:T(8,128)(2,1)} %bitcast.5), calls=%async_computation | async-start | bytes 1114112 | tf_op jit(solution)/shard_map/all_to_all | solution.py:369
  12.6 12.6 %collective-permute-start.2 = (bf16[544,128]{1,0:T(8,128)(2,1)S(1)}, bf16[544,128]{1,0:T(8,128)(2,1)S(1)}, u32[]{:S(2)}, u32[]{:S(2)}) collective-permute-start(bf16[544,128]{1,0:T(8,128)(2,1)S(1)} %get-tuple-element.39), channel_id=1, source_target_pairs={{0,6},{2,4},{4,2},{6,0},{1,7},{3,5},{5,3},{7,1},{8,14},{10,12},{12... | collective-permute-start | bytes 417800 | tf_op jit(solution)/shard_map/ppermute | solution.py:373
  25.3 10.7 %collective-permute-start.3 = (bf16[1056,128]{1,0:T(8,128)(2,1)S(1)}, bf16[1056,128]{1,0:T(8,128)(2,1)S(1)}, u32[]{:S(2)}, u32[]{:S(2)}) collective-permute-start(bf16[1056,128]{1,0:T(8,128)(2,1)S(1)} %join.1.joined_ref), channel_id=1, source_target_pairs={{0,2},{2,0},{4,6},{6,4},{1,3},{3,1},{5,7},{7,5},{8,10},{10,8},{12,... | collective-permute-start | bytes 811016 | tf_op jit(solution)/shard_map/ppermute | solution.py:373
  25.4 21.8 %copy-start.1 = (bf16[1024,352]{0,1:T(8,128)(2,1)S(1)}, bf16[1024,352]{0,1:T(8,128)(2,1)}, u32[]{:S(2)}) copy-start(bf16[1024,352]{0,1:T(8,128)(2,1)} %param.29) | copy-start | bytes 2162692
  25.4 21.8 %copy-start.2 = (bf16[1024,352]{0,1:T(8,128)(2,1)S(1)}, bf16[1024,352]{0,1:T(8,128)(2,1)}, u32[]{:S(2)}) copy-start(bf16[1024,352]{0,1:T(8,128)(2,1)} %param.30) | copy-start | bytes 2162692
  47.2 4.3 %copy-start.3 = (bf16[352,1024]{1,0:T(8,128)(2,1)S(1)}, bf16[352,1024]{1,0:T(8,128)(2,1)}, u32[]{:S(2)}) copy-start(bf16[352,1024]{1,0:T(8,128)(2,1)} %w_ref.1) | copy-start | bytes 2162692
  47.7 3.7 %collective-permute-start.4 = (bf16[712,128]{1,0:T(8,128)(2,1)S(1)}, bf16[712,128]{1,0:T(8,128)(2,1)S(1)}, u32[]{:S(2)}, u32[]{:S(2)}) collective-permute-start(bf16[712,128]{1,0:T(8,128)(2,1)S(1)} %get-tuple-element.43), channel_id=1, source_target_pairs={{0,1},{1,0},{2,3},{3,2},{4,5},{5,4},{6,7},{7,6},{8,9},{9,8},{10,11... | collective-permute-start | bytes 546824 | tf_op jit(solution)/shard_map/ppermute | solution.py:364
